TPU v7x, 32 devices: a whole 2x2x4 slice. The times are simulated.
32 devices in a mesh: sp: 4 (over z), fs: 4 (over y, x), tp: 2 (over core).
Axes of the slice: x: 2, y: 2, z: 4, core: 2. Of those that a mesh axis runs over, the one named last changes fastest.
Arguments:
- tokens: bfloat16 [4, 1024, 2048], P('fs', 'sp', 'tp'), may hold values from -6 to 6
- norm_gain: float32 [2048], replicated, may hold values from 0.1 to 1.9
- query_weight: bfloat16 [2048, 1024], P('fs', 'tp'), may hold values from -1 to 1
- key_weight: bfloat16 [2048, 1024], P('fs', 'tp'), may hold values from -4 to 4
- value_weight: bfloat16 [2048, 1024], P('fs', 'tp'), may hold values from -0.125 to 0.125
- state_query: bfloat16 [2048, 1024], P('fs', 'tp'), may hold values from -0.125 to 0.125
- state_key: bfloat16 [2048, 1024], P('fs', 'tp'), may hold values from -0.125 to 0.125
- state_value: bfloat16 [2048, 1024], P('fs', 'tp'), may hold values from -0.125 to 0.125
- map_lambda: float32 [8], P('tp'), may hold values from 0.3 to 0.8
- diff_gain: float32 [1024], P('tp'), may hold values from 0.1 to 1.9
- decay_rate: float32 [8], P('tp'), may hold values from 0 to 0.04
- state_gain: float32 [1024], P('tp'), may hold values from 0.1 to 1.9
- out_weight: bfloat16 [2048, 2048], replicated, may hold values from -0.125 to 0.125
Outputs:
- mixed: bfloat16 [4, 1024, 2048], P('fs', ('sp', 'tp'))
All inputs are finite; a program needn't handle non-finite values.
Results may differ from a plain program's by a relative error of at most 0.015.
Values may be sent and summed in bfloat16 or wider, within the bound.
A program may use at most 128 MiB of HBM per device.

v0:
```python
import jax
import jax.numpy as jnp
from jax import lax
from jax.sharding import PartitionSpec as P

DK = 64
DV = 128
DR = 128


epsilon = 1e-05
branch_scale = 0.8
masked_score = -1e30


def from_behind(x, axis, by):
    size = lax.axis_size(axis)
    pairs = [(i, i + by) for i in range(size) if 0 <= i + by < size]
    return lax.ppermute(x, axis, pairs)


def entering(x, axis, join, neutral):
    place = lax.axis_index(axis)
    gathered = jax.tree.map(
        lambda a, kind: lax.all_gather(a.astype(kind), axis), x, (jnp.bfloat16, jnp.bfloat16)
    )
    state = jax.tree.map(lambda a, e: jnp.zeros_like(a) + jnp.asarray(e, a.dtype), x, neutral)

    def one(turn, state):
        return join(
            state,
            jax.tree.map(
                lambda a, own: lax.dynamic_index_in_dim(a, turn, 0, False).astype(own.dtype),
                gathered,
                x,
            ),
        )

    return lax.fori_loop(0, place, one, state)


def attend(att_query, att_keys, att_values, map_lambda, diff_gain):
    tok_rows = att_query.shape[0]
    head_count = map_lambda.shape[0]
    key_width = att_keys.shape[1]
    query_heads = att_query.reshape(tok_rows, head_count, 2, DK)
    sp_index = lax.axis_index("sp")
    query_place = sp_index * tok_rows + jnp.arange(tok_rows)
    score_scale = DK ** (-0.5)

    def absorb_block(running, inputs):
        key_block, key_place = inputs
        key_heads = key_block[:, :key_width].reshape(tok_rows, head_count, 2, DK)
        value_heads = key_block[:, key_width:].reshape(tok_rows, head_count, DV)
        scores = (
            jnp.einsum(
                "qhmd,khmd->mhqk", query_heads, key_heads, preferred_element_type=jnp.float32
            )
            * score_scale
        )
        causal = key_place[None, :] <= query_place[:, None]
        row_peak, totals, summed = running
        new_peak = jnp.maximum(row_peak, jnp.max(jnp.where(causal, scores, masked_score), axis=-1))
        weights = jnp.where(causal, jnp.exp(scores - new_peak[..., None]), 0.0)
        factor = jnp.exp(row_peak - new_peak)
        totals = totals * factor + jnp.sum(weights, axis=-1)
        summed = summed * factor[..., None] + jnp.einsum(
            "mhqk,khv->mhqv",
            weights.astype(jnp.bfloat16),
            value_heads,
            preferred_element_type=jnp.float32,
        )
        return ((new_peak, totals, summed), None)

    def absorb(running, pieces, first_row):
        piece_rows = pieces.shape[0]
        stacked = pieces.reshape(piece_rows // tok_rows, tok_rows, pieces.shape[1])
        places = (first_row + jnp.arange(piece_rows)).reshape(piece_rows // tok_rows, tok_rows)
        return lax.scan(absorb_block, running, (stacked, places))[0]

    starting = (
        jnp.full((2, head_count, tok_rows), masked_score, jnp.float32),
        jnp.zeros((2, head_count, tok_rows), jnp.float32),
        jnp.zeros((2, head_count, tok_rows, DV), jnp.float32),
    )
    joined_kv = jnp.concatenate([att_keys, att_values], axis=1)
    first_state = absorb(starting, joined_kv, sp_index * tok_rows)

    def relay_step(step_index, relay_state):
        running, moving = relay_state
        moving = from_behind(moving, "sp", 1)
        first_row = (sp_index - step_index) * tok_rows
        running = lax.cond(
            first_row >= 0,
            lambda holding: absorb(holding, moving, first_row),
            lambda holding: holding,
            running,
        )
        return (running, moving)

    running, _ = lax.fori_loop(1, lax.axis_size("sp"), relay_step, (first_state, joined_kv))
    row_peak, totals, summed = running
    averaged = summed / totals[..., None]
    differ = averaged[0] - map_lambda[:, None, None] * averaged[1]
    normed = differ * lax.rsqrt(jnp.mean(differ * differ, axis=-1, keepdims=True) + epsilon)
    normed = normed * diff_gain.reshape(head_count, 1, DV) * branch_scale
    return normed.transpose(1, 0, 2).reshape(tok_rows, head_count * DV).astype(jnp.bfloat16)


def retain(ret_query, ret_keys, ret_values, decay_rate, state_gain):
    tok_rows = ret_query.shape[0]
    head_count = decay_rate.shape[0]
    query_heads = ret_query.reshape(tok_rows, head_count, DR)
    key_heads = ret_keys.reshape(tok_rows, head_count, DR)
    value_heads = ret_values.reshape(tok_rows, head_count, DR)
    position = jnp.arange(tok_rows).astype(jnp.float32)
    distance = position[:, None] - position[None, :]
    decay_col = decay_rate[:, None, None]
    within = jnp.where(distance >= 0, jnp.exp(-decay_col * jnp.maximum(distance, 0.0)), 0.0)
    local_scores = (
        jnp.einsum("qhd,khd->hqk", query_heads, key_heads, preferred_element_type=jnp.float32)
        * within
    )
    intra_out = jnp.einsum(
        "hqk,khv->hqv",
        local_scores.astype(jnp.bfloat16),
        value_heads,
        preferred_element_type=jnp.float32,
    )
    key_decayed = key_heads.astype(jnp.float32) * jnp.exp(
        -decay_rate[None, :, None] * (tok_rows - 1.0 - position)[:, None, None]
    )
    own_state = jnp.einsum(
        "khd,khv->hdv",
        key_decayed,
        value_heads.astype(jnp.float32),
        precision=lax.Precision.HIGHEST,
    )
    block_decay = jnp.exp(-decay_rate * tok_rows)

    def link_states(earlier, later):
        return (earlier[0] * later[1][:, None, None] + later[0], earlier[1] * later[1])

    identity = (jnp.zeros_like(own_state), jnp.ones_like(block_decay))
    incoming, _ = entering((own_state, block_decay), "sp", link_states, identity)
    carried = jnp.einsum(
        "qhd,hdv->hqv", query_heads.astype(jnp.float32), incoming, precision=lax.Precision.HIGHEST
    )
    carried = carried * jnp.exp(-decay_col * (position + 1.0)[None, :, None])
    combined = intra_out + carried
    normed = combined * lax.rsqrt(jnp.mean(combined * combined, axis=-1, keepdims=True) + epsilon)
    normed = normed * state_gain.reshape(head_count, 1, DR)
    return normed.transpose(1, 0, 2).reshape(tok_rows, head_count * DR).astype(jnp.bfloat16)


def body(
    tokens,
    norm_gain,
    query_weight,
    key_weight,
    value_weight,
    state_query,
    state_key,
    state_value,
    map_lambda,
    diff_gain,
    decay_rate,
    state_gain,
    out_weight,
):
    gathered = lax.all_gather(tokens[0], "tp", axis=1, tiled=True)
    tok_float = gathered.astype(jnp.float32)
    normed = tok_float * lax.rsqrt(
        jnp.mean(tok_float * tok_float, axis=-1, keepdims=True) + epsilon
    )
    normed = (normed * norm_gain).astype(jnp.bfloat16)
    pieces = (
        lax.all_gather(query_weight, "fs", axis=0, tiled=True),
        lax.all_gather(key_weight, "fs", axis=0, tiled=True),
        lax.all_gather(value_weight, "fs", axis=0, tiled=True),
        lax.all_gather(state_query, "fs", axis=0, tiled=True),
        lax.all_gather(state_key, "fs", axis=0, tiled=True),
        lax.all_gather(state_value, "fs", axis=0, tiled=True),
    )
    projected = tuple(
        (jnp.dot(normed, row_block, preferred_element_type=jnp.float32) for row_block in pieces)
    )
    att_query, att_keys, att_values, ret_query, ret_keys, ret_values = (
        member.astype(jnp.bfloat16) for member in projected
    )
    attended = attend(att_query, att_keys, att_values, map_lambda, diff_gain)
    retained = retain(ret_query, ret_keys, ret_values, decay_rate, state_gain)
    joined = jnp.concatenate([attended, retained], axis=1)
    diff_width = attended.shape[1]
    ret_width = retained.shape[1]
    tp_count = lax.axis_size("tp")
    tp_index = lax.axis_index("tp")
    own_rows = jnp.concatenate(
        [
            lax.dynamic_slice_in_dim(out_weight, tp_index * diff_width, diff_width, 0),
            lax.dynamic_slice_in_dim(
                out_weight, tp_count * diff_width + tp_index * ret_width, ret_width, 0
            ),
        ],
        axis=0,
    )
    output = lax.psum_scatter(
        jnp.dot(joined, own_rows, preferred_element_type=jnp.float32).astype(jnp.bfloat16),
        "tp",
        scatter_dimension=0,
        tiled=True,
    )
    return output[None]


def solution(mesh):
    placed = (
        P("fs", "sp", "tp"),
        P(),
        P("fs", "tp"),
        P("fs", "tp"),
        P("fs", "tp"),
        P("fs", "tp"),
        P("fs", "tp"),
        P("fs", "tp"),
        P("tp"),
        P("tp"),
        P("tp"),
        P("tp"),
        P(),
    )
    return jax.shard_map(
        body, mesh=mesh, in_specs=placed, out_specs=P("fs", ("sp", "tp"), None), check_vma=False
    )
```

profile of v0, /device:TPU:15, one launch (start us, length us, event | category | flops | bytes accessed | tf_op | source)
XLA Modules:
  0.0 269.5 jit_solution(17242636833835329736)
XLA Ops:
  6.5 0.7 all-gather.23.cloned.1.call-update
  7.3 0.7 all-gather.11.cloned.1.call-update
  8.1 0.7 all-gather.13.cloned.1.call-update
  8.8 0.5 all-gather.15.cloned.1.call-update
  9.4 0.5 all-gather.19.cloned.1.call-update
  10.0 0.5 all-gather.21.cloned.1.call-update
  10.5 0.7 all-gather.17.cloned.1.call-update
  11.3 0.8 subtract_maximum_fusion
  12.1 0.1 subtract_compare_fusion
  12.6 0.6 dynamic-slice.4
  13.8 0.2 dynamic-update-slice
  14.1 7.2 %all-reduce = bf16[16]{0:T(256)(128)(2,1)S(1)} all-reduce(bf16[16]{0:T(256)(128)(2,1)S(1)} %dynamic-update-slice), channel_id=3, replica_groups=mesh['sp'=4,'fs'=4,'tp'=2] {'sp'}, use_global_device_ids=true, to_apply=%add | all-reduce | flops 16 | bytes 64
  21.4 4.8 %constant_dynamic-slice_fusion.1 = (bf16[512,2048]{1,0:T(8,128)(2,1)}, bf16[512,2048]{1,0:T(8,128)(2,1)}) fusion(bf16[2048,2048]{1,0:T(8,128)(2,1)} %param.31, s32[]{:T(128)S(6)} %select_n.37, s32[]{:T(128)S(6)} %select_n.38), kind=kLoop, calls=%fused_computation.101 | loop fusion | bytes 8388616 | tf_op jit(solution)/shard_map/dynamic_slice | solution.py:200
  26.2 1.5 fusion.15
  27.7 28.5 %all-gather.11.cloned.1.call-done = bf16[2048,512]{1,0:T(8,128)(2,1)} async-done(((bf16[512,512]{1,0:T(8,128)(2,1)}), bf16[2048,512]{1,0:T(8,128)(2,1)}) %all-gather.11.cloned.1.call-update) | async-done | bytes 2097168 | tf_op jit(solution)/shard_map/all_gather | solution.py:178
  56.2 2.7 convolution_convert_fusion.5
  58.9 0.1 copy.54
  59.0 34.2 %all-gather.13.cloned.1.call-done = bf16[2048,512]{1,0:T(8,128)(2,1)} async-done(((bf16[512,512]{1,0:T(8,128)(2,1)}), bf16[2048,512]{1,0:T(8,128)(2,1)}) %all-gather.13.cloned.1.call-update) | async-done | bytes 2097168 | tf_op jit(solution)/shard_map/all_gather | solution.py:179
  93.2 2.3 convolution_convert_fusion.4
  95.6 0.1 copy.55
  95.7 0.5 select_reduce_fusion.1
  96.3 0.5 fusion.18
  96.8 33.3 %all-gather.15.cloned.1.call-done = bf16[2048,512]{1,0:T(8,128)(2,1)} async-done(((bf16[512,512]{1,0:T(8,128)(2,1)}), bf16[2048,512]{1,0:T(8,128)(2,1)}) %all-gather.15.cloned.1.call-update) | async-done | bytes 2097168 | tf_op jit(solution)/shard_map/all_gather | solution.py:180
  130.2 2.3 convolution_convert_fusion.3
  132.5 0.1 copy.80
  132.6 0.6 copy-done.4
  133.2 0.3 fusion.20
  133.5 0.6 copy-done.5
  134.2 0.3 copy.61
  134.6 0.2 copy.62
  134.8 44.7 %while.26 = (s32[]{:T(128)}, f32[2,4,256]{2,1,0:T(4,128)S(1)}, f32[2,4,256]{2,1,0:T(4,128)S(1)}, f32[2,4,256,128]{3,2,0,1:T(8,128)S(1)}, bf16[256,1024]{0,1:T(8,...) while((s32[]{:T(128)}, f32[2,4,256]{2,1,0:T(4,128)S(1)}, ...), condition=%wide.region_8.9_spmd.clone, body=%wide.region_3.8_spmd.clone.sunk | while | flops 206115328 | bytes 13711675 | solution.py:101
  134.8 3.1 %collective-permute-start = (bf16[256,1024]{0,1:T(8,128)(2,1)S(1)}, bf16[256,1024]{0,1:T(8,128)(2,1)S(1)}, u32[]{:S(2)}, u32[]{:S(2)}) collective-permute-start(bf16[256,1024]{0,1:T(8,128)(2,1)S(1)} %get-tuple-element.509), channel_id=1, source_target_pairs={{0,8},{8,16},{16,24},{1,9},{9,17},{17,25},{2,10},{10,18},{18,26},{... | collective-permute-start | bytes 1572872 | tf_op jit(solution)/shard_map/while/body/eval_jaxpr/ppermute | solution.py:19
  137.9 11.4 %collective-permute-done = bf16[256,1024]{0,1:T(8,128)(2,1)S(1)} collective-permute-done((bf16[256,1024]{0,1:T(8,128)(2,1)S(1)}, bf16[256,1024]{0,1:T(8,128)(2,1)S(1)}, u32[]{:S(2)}, u32[]{:S(2)}) %collective-permute-start) | collective-permute-done | bytes 524320 | tf_op jit(solution)/shard_map/while/body/eval_jaxpr/ppermute | solution.py:19
  149.3 2.2 conditional.3
  149.5 0.5 select_reduce_fusion
  150.0 0.5 fusion.2
  150.6 0.9 fusion.4
  151.5 3.1 %collective-permute-start = (bf16[256,1024]{0,1:T(8,128)(2,1)S(1)}, bf16[256,1024]{0,1:T(8,128)(2,1)S(1)}, u32[]{:S(2)}, u32[]{:S(2)}) collective-permute-start(bf16[256,1024]{0,1:T(8,128)(2,1)S(1)} %get-tuple-element.509), channel_id=1, source_target_pairs={{0,8},{8,16},{16,24},{1,9},{9,17},{17,25},{2,10},{10,18},{18,26},{... | collective-permute-start | bytes 1572872 | tf_op jit(solution)/shard_map/while/body/eval_jaxpr/ppermute | solution.py:19
  154.7 10.6 %collective-permute-done = bf16[256,1024]{0,1:T(8,128)(2,1)S(1)} collective-permute-done((bf16[256,1024]{0,1:T(8,128)(2,1)S(1)}, bf16[256,1024]{0,1:T(8,128)(2,1)S(1)}, u32[]{:S(2)}, u32[]{:S(2)}) %collective-permute-start) | collective-permute-done | bytes 524320 | tf_op jit(solution)/shard_map/while/body/eval_jaxpr/ppermute | solution.py:19
  165.4 5.3 %collective-permute-start = (bf16[256,1024]{0,1:T(8,128)(2,1)S(1)}, bf16[256,1024]{0,1:T(8,128)(2,1)S(1)}, u32[]{:S(2)}, u32[]{:S(2)}) collective-permute-start(bf16[256,1024]{0,1:T(8,128)(2,1)S(1)} %get-tuple-element.509), channel_id=1, source_target_pairs={{0,8},{8,16},{16,24},{1,9},{9,17},{17,25},{2,10},{10,18},{18,26},{... | collective-permute-start | bytes 1572872 | tf_op jit(solution)/shard_map/while/body/eval_jaxpr/ppermute | solution.py:19
  170.7 8.8 %collective-permute-done = bf16[256,1024]{0,1:T(8,128)(2,1)S(1)} collective-permute-done((bf16[256,1024]{0,1:T(8,128)(2,1)S(1)}, bf16[256,1024]{0,1:T(8,128)(2,1)S(1)}, u32[]{:S(2)}, u32[]{:S(2)}) %collective-permute-start) | collective-permute-done | bytes 524320 | tf_op jit(solution)/shard_map/while/body/eval_jaxpr/ppermute | solution.py:19
  179.5 0.3 copy.64
  179.9 0.8 copy-done.3
  180.8 2.3 convolution_convert_fusion.1
  183.1 0.1 copy.82
  183.4 0.4 copy-done.11
  183.8 0.2 multiply_reduce_fusion.1
  183.9 20.1 %all-gather.21.cloned.1.call-done = bf16[2048,512]{1,0:T(8,128)(2,1)} async-done(((bf16[512,512]{1,0:T(8,128)(2,1)}), bf16[2048,512]{1,0:T(8,128)(2,1)}) %all-gather.21.cloned.1.call-update) | async-done | bytes 2097168 | tf_op jit(solution)/shard_map/all_gather | solution.py:183
  204.0 2.3 fusion.24
  206.3 0.7 copy-done.15
  207.0 0.4 convolution_convert_fusion.6
  207.4 12.4 %all-gather.2 = bf16[16,128,128]{2,1,0:T(8,128)(2,1)S(1)} all-gather(bf16[4,128,128]{2,1,0:T(8,128)(2,1)S(1)} %convolution_convert_fusion.6), channel_id=4, replica_groups=mesh['sp'=4,'fs'=4,'tp'=2] {'sp'}, dimensions={0}, use_global_device_ids=true | all-gather | bytes 655360 | tf_op jit(solution)/shard_map/all_gather | solution.py:25
  219.9 0.3 while.25
  219.9 0.1 convert_add_fusion.2
  220.2 20.8 %all-gather.17.cloned.1.call-done = bf16[2048,512]{1,0:T(8,128)(2,1)} async-done(((bf16[512,512]{1,0:T(8,128)(2,1)}), bf16[2048,512]{1,0:T(8,128)(2,1)}) %all-gather.17.cloned.1.call-update) | async-done | bytes 2097168 | tf_op jit(solution)/shard_map/all_gather | solution.py:181
  241.0 2.3 fusion.23
  243.4 0.7 copy-done.8
  244.1 1.2 fusion.46
  245.3 2.8 %multiply_reduce_fusion = (f32[4,256]{1,0:T(4,128)S(1)}, f32[4,256,128]{1,2,0:T(8,128)}) fusion(f32[4,256,128]{1,2,0:T(8,128)} %fusion.46, f32[4,256]{1,0:T(4,128)S(1)} %multiply_exponential_fusion, bf16[32,4,8,128]{3,2,1,0:T(8,128)(2,1)} %copy-done.15, bf16[256,4,128]{0,2,1:T(8,128)(2,1)} %bitcast.134, f32[256,256]{1,0:T(8,128)S(1)} %copy-done.6, ...), kind=kOutput, calls=%fused_computation.62 | convolution fusion | flops 135789568 | bytes 2170896 | tf_op jit(solution)/shard_map/hqk,khv->hqv/dot_general | solution.py:124
  248.1 0.2 multiply_convert_fusion
  248.3 1.4 fusion.37
  249.7 0.2 copy-done.1
  250.0 2.3 fusion.12
  252.3 10.4 %reduce-scatter.2.cloned.1.call-done = bf16[128,2048]{1,0:T(8,128)(2,1)} async-done(((bf16[256,2048]{1,0:T(8,128)(2,1)}), bf16[128,2048]{1,0:T(8,128)(2,1)}) %reduce-scatter.2.cloned.1.call-update) | async-done | bytes 524304 | tf_op jit(solution)/shard_map/reduce_scatter | solution.py:207
  (72 shorter events, 1.3 us)
Async XLA Ops:
  6.5 6.0 %copy-start.14 = (u32[32]{0:T(128)S(1)}, u32[32]{0:T(128)}, u32[]{:S(2)}) copy-start(u32[32]{0:T(128)} %constant.126) | copy-start | bytes 388
  6.5 5.8 %copy-start.13 = (f32[4]{0:T(128)S(1)}, f32[4]{0:T(128)}, u32[]{:S(2)}) copy-start(f32[4]{0:T(128)} %param.29) | copy-start | bytes 52
  6.5 19.6 %all-gather.23.cloned.1.call-start = ((), (), s32[]{:S(2)}) async-start(), calls=%async_computation.8 | async-start | bytes 1572864 | tf_op jit(solution)/shard_map/all_gather | solution.py:171
  7.3 48.9 %all-gather.11.cloned.1.call-start = ((), (), s32[]{:S(2)}) async-start(), calls=%async_computation.1 | async-start | bytes 2621440 | tf_op jit(solution)/shard_map/all_gather | solution.py:178
  8.0 85.2 %all-gather.13.cloned.1.call-start = ((), (), s32[]{:S(2)}) async-start(), calls=%async_computation.2 | async-start | bytes 2621440 | tf_op jit(solution)/shard_map/all_gather | solution.py:179
  8.7 121.4 %all-gather.15.cloned.1.call-start = ((), (), s32[]{:S(2)}) async-start(), calls=%async_computation.3 | async-start | bytes 2621440 | tf_op jit(solution)/shard_map/all_gather | solution.py:180
  9.3 170.6 %all-gather.19.cloned.1.call-start = ((), (), s32[]{:S(2)}) async-start(), calls=%async_computation.5 | async-start | bytes 2621440 | tf_op jit(solution)/shard_map/all_gather | solution.py:182
  9.9 194.1 %all-gather.21.cloned.1.call-start = ((), (), s32[]{:S(2)}) async-start(), calls=%async_computation.6 | async-start | bytes 2621440 | tf_op jit(solution)/shard_map/all_gather | solution.py:183
  10.5 230.5 %all-gather.17.cloned.1.call-start = ((), (), s32[]{:S(2)}) async-start(), calls=%async_computation.4 | async-start | bytes 2621440 | tf_op jit(solution)/shard_map/all_gather | solution.py:181
  11.2 251.4 %reduce-scatter.2.cloned.1.call-start = ((), (), s32[]{:S(2)}) async-start(), calls=%async_computation.7 | async-start | bytes 1572864 | tf_op jit(solution)/shard_map/reduce_scatter | solution.py:207
  21.4 34.8 %copy-start.12 = (f32[2048]{0:T(1024)S(1)}, f32[2048]{0:T(1024)}, u32[]{:S(2)}) copy-start(f32[2048]{0:T(1024)} %param.20) | copy-start | bytes 24580
  27.7 65.6 %copy-start.2 = (bf16[1,256,2048]{2,1,0:T(8,128)(2,1)S(1)}, bf16[1,256,2048]{2,1,0:T(8,128)(2,1)}, u32[]{:S(2)}) copy-start(bf16[1,256,2048]{2,1,0:T(8,128)(2,1)} %all-gather.23.cloned.1.call-done) | copy-start | bytes 3145732
  132.5 0.7 copy-start.4
  133.2 0.9 copy-start.5
  134.8 14.5 %collective-permute-start = (bf16[256,1024]{0,1:T(8,128)(2,1)S(1)}, bf16[256,1024]{0,1:T(8,128)(2,1)S(1)}, u32[]{:S(2)}, u32[]{:S(2)}) collective-permute-start(bf16[256,1024]{0,1:T(8,128)(2,1)S(1)} %get-tuple-element.509), channel_id=1, source_target_pairs={{0,8},{8,16},{16,24},{1,9},{9,17},{17,25},{2,10},{10,18},{18,26},{... | collective-permute-start | bytes 1572872 | tf_op jit(solution)/shard_map/while/body/eval_jaxpr/ppermute | solution.py:19
  151.5 13.8 %collective-permute-start = (bf16[256,1024]{0,1:T(8,128)(2,1)S(1)}, bf16[256,1024]{0,1:T(8,128)(2,1)S(1)}, u32[]{:S(2)}, u32[]{:S(2)}) collective-permute-start(bf16[256,1024]{0,1:T(8,128)(2,1)S(1)} %get-tuple-element.509), channel_id=1, source_target_pairs={{0,8},{8,16},{16,24},{1,9},{9,17},{17,25},{2,10},{10,18},{18,26},{... | collective-permute-start | bytes 1572872 | tf_op jit(solution)/shard_map/while/body/eval_jaxpr/ppermute | solution.py:19
  165.4 14.1 %collective-permute-start = (bf16[256,1024]{0,1:T(8,128)(2,1)S(1)}, bf16[256,1024]{0,1:T(8,128)(2,1)S(1)}, u32[]{:S(2)}, u32[]{:S(2)}) collective-permute-start(bf16[256,1024]{0,1:T(8,128)(2,1)S(1)} %get-tuple-element.509), channel_id=1, source_target_pairs={{0,8},{8,16},{16,24},{1,9},{9,17},{17,25},{2,10},{10,18},{18,26},{... | collective-permute-start | bytes 1572872 | tf_op jit(solution)/shard_map/while/body/eval_jaxpr/ppermute | solution.py:19
  179.5 1.2 copy-start.3
  183.1 0.7 copy-start.11
  183.2 23.1 %copy-start.7 = (bf16[256,512]{0,1:T(8,128)(2,1)}, bf16[256,512]{0,1:T(8,128)(2,1)S(1)}, u32[]{:S(2)}) copy-start(bf16[256,512]{0,1:T(8,128)(2,1)S(1)} %copy.82) | copy-start | bytes 786436
  206.3 0.7 copy-start.15
  220.2 25.1 %copy-start.6 = (f32[256,256]{1,0:T(8,128)S(1)}, f32[256,256]{1,0:T(8,128)}, u32[]{:S(2)}) copy-start(f32[256,256]{1,0:T(8,128)} %subtract_maximum_fusion) | copy-start | bytes 786436
  243.4 0.7 copy-start.8
  243.4 4.7 %copy-start.9 = (f32[512]{0:T(512)S(1)}, f32[512]{0:T(512)}, u32[]{:S(2)}) copy-start(f32[512]{0:T(512)} %param.28) | copy-start | bytes 6148
  245.3 3.0 %copy-start.10 = (f32[512]{0:T(512)S(1)}, f32[512]{0:T(512)}, u32[]{:S(2)}) copy-start(f32[512]{0:T(512)} %param.30) | copy-start | bytes 6148
  245.3 4.5 %copy-start = (bf16[512,2048]{1,0:T(8,128)(2,1)S(1)}, bf16[512,2048]{1,0:T(8,128)(2,1)}, u32[]{:S(2)}) copy-start(bf16[512,2048]{1,0:T(8,128)(2,1)} %get-tuple-element.361) | copy-start | bytes 6291460
  248.1 1.9 copy-start.1
Sparse Core Ops, SparseCore 0:
  8.9 10.8 all-gather.22
  21.6 34.5 all-gather.10
  58.0 35.1 all-gather.12
  94.9 35.1 all-gather.14
  131.8 35.1 all-gather.18
  168.8 35.1 all-gather.20
  205.8 35.1 all-gather.16
  252.4 10.2 reduce-scatter.1
where the time goes:
time: 271 us; the launch traced here: 269 us
  waiting for transfers between devices  183 us (68%)
  matrix products  23.3 us (9%)
  blocking collectives  19.6 us (7%)
  between operations  14.5 us (5%)
  starting transfers between devices  11.8 us (4%)
  local copies, waits for them, and re-layouts  11.4 us (4%)
  other arithmetic  5.94 us (2%)
    all_gather x1, waiting for transfers between devices, body(): lax.all_gather(key_weight, 'fs', axis=0, tiled=True)  34.2 us
    all_gather x1, waiting for transfers between devices, body(): lax.all_gather(value_weight, 'fs', axis=0, tiled=True)  33.3 us
    ppermute x3, waiting for transfers between devices, from_behind(): return lax.ppermute(x, axis, pairs)  30.8 us
    all_gather x1, waiting for transfers between devices, body(): lax.all_gather(query_weight, 'fs', axis=0, tiled=True)  28.5 us
    all_gather x1, waiting for transfers between devices, body(): lax.all_gather(state_query, 'fs', axis=0, tiled=True)  20.8 us
    all_gather x1, waiting for transfers between devices, body(): lax.all_gather(state_value, 'fs', axis=0, tiled=True)  20.1 us
    dot_general x6, matrix products, body(): jnp.dot(normed, row_block, preferred_element_type=jnp.float32)  14.3 us
    all_gather x1, blocking collectives, entering(): lax.all_gather(a.astype(kind), axis)  12.4 us
  transfers between devices with their start and end apart: 11, of which 9 were waited for; matrix products, arithmetic and copies ran while one was open for 10% of the time, Pallas kernels for 0%

commit v1 on v0

--- a/solution.py
+++ b/solution.py
@@ -1,6 +1,10 @@
+import functools
+
 import jax
 import jax.numpy as jnp
 from jax import lax
+from jax.experimental import pallas as pl
+from jax.experimental.pallas import tpu as pltpu
 from jax.sharding import PartitionSpec as P
 
 DK = 64
@@ -153,7 +157,7 @@
     return normed.transpose(1, 0, 2).reshape(tok_rows, head_count * DR).astype(jnp.bfloat16)
 
 
-def body(
+def spread_body(
     tokens,
     norm_gain,
     query_weight,
@@ -213,6 +217,133 @@
     return output[None]
 
 
+def row_product(a, b):
+    return lax.dot_general(a, b, (((1,), (1,)), ((), ())), preferred_element_type=jnp.float32)
+
+
+def mixers_kernel(block, heads, proj, lam_ref, dgain_ref, rate_ref, sgain_ref, out):
+    length = proj.shape[0]
+    group = heads * DV
+    f32, bf16 = jnp.float32, jnp.bfloat16
+    row = lax.broadcasted_iota(jnp.int32, (block, block), 0)
+    col = lax.broadcasted_iota(jnp.int32, (block, block), 1)
+    causal = col <= row
+    lane = lax.broadcasted_iota(jnp.int32, (block, 2 * DK), 1)
+    position = lax.broadcasted_iota(jnp.int32, (block, 1), 0).astype(f32)
+
+    def part(kind, head, first, count):
+        return proj[first : first + count, kind * group + head * DV : kind * group + head * DV + DV]
+
+    for head in range(heads):
+        spot = slice(head * DV, head * DV + DV)
+        lam = lam_ref[:, head : head + 1]
+        rate = rate_ref[:, head : head + 1]
+        gain = dgain_ref[:, spot] * branch_scale
+        within = jnp.where(causal, jnp.exp(-rate * jnp.maximum(row - col, 0).astype(f32)), 0.0)
+        query_decay = jnp.exp(-rate * (position + 1.0))
+        key_decay = jnp.exp(-rate * (block - 1.0 - position))
+        block_decay = jnp.exp(-rate * block)
+        state = jnp.zeros((DR, DR), f32)
+        for turn in range(length // block):
+            first = turn * block
+            query = part(0, head, first, block) * jnp.asarray(DK ** (-0.5), bf16)
+            averaged = []
+            for which in range(2):
+                own = jnp.where((lane >= DK) == bool(which), query, jnp.zeros_like(query))
+                near = jnp.where(causal, row_product(own, part(1, head, first, block)), masked_score)
+                peak = jnp.max(near, axis=1, keepdims=True)
+                if first:
+                    far = row_product(own, part(1, head, 0, first))
+                    peak = jnp.maximum(peak, jnp.max(far, axis=1, keepdims=True))
+                near = jnp.exp(near - peak)
+                total = jnp.sum(near, axis=1, keepdims=True)
+                summed = jnp.dot(near.astype(bf16), part(2, head, first, block), preferred_element_type=f32)
+                if first:
+                    far = jnp.exp(far - peak)
+                    total = total + jnp.sum(far, axis=1, keepdims=True)
+                    summed = summed + jnp.dot(
+                        far.astype(bf16), part(2, head, 0, first), preferred_element_type=f32
+                    )
+                averaged.append(summed / total)
+            differ = averaged[0] - lam * averaged[1]
+            scaled = differ * lax.rsqrt(jnp.mean(differ * differ, axis=1, keepdims=True) + epsilon)
+            out[first : first + block, spot] = (scaled * gain).astype(bf16)
+            ret_query = part(3, head, first, block)
+            ret_keys = part(4, head, first, block)
+            ret_values = part(5, head, first, block)
+            local = (row_product(ret_query, ret_keys) * within).astype(bf16)
+            mixed = jnp.dot(local, ret_values, preferred_element_type=f32)
+            if first:
+                mixed = mixed + query_decay * jnp.dot(
+                    ret_query, state.astype(bf16), preferred_element_type=f32
+                )
+            if first + block < length:
+                decayed = (ret_keys.astype(f32) * key_decay).astype(bf16)
+                state = state * block_decay + lax.dot_general(
+                    decayed, ret_values, (((0,), (0,)), ((), ())), preferred_element_type=f32
+                )
+            scaled = mixed * lax.rsqrt(jnp.mean(mixed * mixed, axis=1, keepdims=True) + epsilon)
+            out[first : first + block, group + head * DV : group + head * DV + DV] = (
+                scaled * sgain_ref[:, spot]
+            ).astype(bf16)
+
+
+def own_heads(x, heads):
+    first = lax.axis_index("sp") * heads
+    return lax.dynamic_slice_in_dim(x, first, heads, 0)[None]
+
+
+def mix(proj, block, heads, map_lambda, diff_gain, decay_rate, state_gain):
+    length = proj.shape[0]
+    vmem = pl.BlockSpec(memory_space=pltpu.VMEM)
+    return pl.pallas_call(
+        functools.partial(mixers_kernel, block, heads),
+        out_shape=jax.ShapeDtypeStruct((length, 2 * heads * DV), jnp.bfloat16),
+        in_specs=[vmem] * 5,
+        out_specs=vmem,
+        compiler_params=pltpu.CompilerParams(vmem_limit_bytes=48 * 1024 * 1024),
+    )(
+        proj,
+        own_heads(map_lambda, heads),
+        own_heads(diff_gain, heads * DV),
+        own_heads(decay_rate, heads),
+        own_heads(state_gain, heads * DR),
+    )
+
+
+def body(tokens, norm_gain, *rest):
+    weights, (map_lambda, diff_gain, decay_rate, state_gain, out_weight) = rest[:6], rest[6:]
+    sp_count = lax.axis_size("sp")
+    tp_count = lax.axis_size("tp")
+    if map_lambda.shape[0] % sp_count or decay_rate.shape[0] != map_lambda.shape[0]:
+        return spread_body(tokens, norm_gain, *rest)
+    heads = map_lambda.shape[0] // sp_count
+    block = tokens.shape[1]
+    width = heads * DV
+    place = lax.axis_index("sp")
+    own = jnp.concatenate(
+        [lax.dynamic_slice_in_dim(w, place * width, width, 1) for w in weights], axis=1
+    )
+    weight = lax.all_gather(own, "fs", axis=0, tiled=True)
+    sequence = lax.all_gather(tokens[0], "sp", axis=0, tiled=True)
+    sequence = lax.all_gather(sequence, "tp", axis=1, tiled=True)
+    tok_float = sequence.astype(jnp.float32)
+    normed = tok_float * lax.rsqrt(
+        jnp.mean(tok_float * tok_float, axis=-1, keepdims=True) + epsilon
+    )
+    normed = (normed * norm_gain).astype(jnp.bfloat16)
+    proj = jnp.dot(normed, weight, preferred_element_type=jnp.float32).astype(jnp.bfloat16)
+    mine = mix(proj, block, heads, map_lambda, diff_gain, decay_rate, state_gain)
+    count = sp_count * tp_count
+    moved = lax.all_to_all(
+        mine.reshape(count, mine.shape[0] // count, mine.shape[1]), ("sp", "tp"), 0, 0, tiled=True
+    )
+    rows = moved.shape[1]
+    joined = moved.reshape(sp_count, tp_count, rows, 2, width).transpose(2, 3, 1, 0, 4)
+    joined = joined.reshape(rows, out_weight.shape[0])
+    return jnp.dot(joined, out_weight, preferred_element_type=jnp.float32).astype(jnp.bfloat16)[None]
+
+
 def solution(mesh):
     placed = (
         P("fs", "sp", "tp"),

time: 271 us -> 162 us (0.60)
  the two profiles are of different devices: /device:TPU:15 before, /device:TPU:0 now
where the time goes in v1:
time: 162 us
  waiting for transfers between devices  100 us (62%)
  blocking collectives  19.7 us (12%)
  between operations  13.2 us (8%)
  matrix products  12.1 us (7%)
  local copies, waits for them, and re-layouts  8.8 us (5%)
  Pallas kernels  5.07 us (3%)
  other arithmetic  3.08 us (2%)
    all_gather x1, waiting for transfers between devices, body(): sequence = lax.all_gather(tokens[0], 'sp', axis=0, tiled=True)  50 us
    all_gather x1, waiting for transfers between devices, body(): weight = lax.all_gather(own, 'fs', axis=0, tiled=True)  43.8 us
    all_to_all x1, blocking collectives, body(): lax.all_to_all(mine.reshape(count, mine.shape[0] // count, mine.shape[1])...  19.7 us
    dot_general x1, matrix products, body(): jnp.dot(normed, weight, preferred_element_type=jnp.float32)  6.63 us
    unnamed x13, local copies, waits for them, and re-layouts  5.6 us
    dot_general x1, matrix products, body(): jnp.dot(joined, out_weight, preferred_element_type=jnp.float32)  5.47 us
    all_gather x1, waiting for transfers between devices, body(): sequence = lax.all_gather(sequence, 'tp', axis=1, tiled=True)  5.42 us
    pallas_call x1, Pallas kernels, mix(): pl.pallas_call(functools.partial(mixers_kernel, block, heads), out_shape=...  5.07 us
  transfers between devices with their start and end apart: 3, of which 3 were waited for; matrix products, arithmetic and copies ran while one was open for 7% of the time, Pallas kernels for 0%

profile of v1, /device:TPU:0, one launch (start us, length us, event | category | flops | bytes accessed | tf_op | source)
XLA Modules:
  0.0 162.0 jit_solution(11160700498352700339)
XLA Ops:
  6.5 0.0 copy-start.2
  6.5 0.0 copy-start.3
  6.5 0.0 all-gather.8.cloned.1.call-start
  6.5 0.7 all-gather.8.cloned.1.call-update
  7.3 0.0 all-gather.10.cloned.1.call-start
  7.3 50.0 %all-gather.8.cloned.1.call-done = bf16[1,1024,1024]{2,1,0:T(8,128)(2,1)} async-done(((bf16[1,256,1024]{2,1,0:T(8,128)(2,1)}), bf16[1,1024,1024]{2,1,0:T(8,128)(2,1)}) %all-gather.8.cloned.1.call-update) | async-done | bytes 2097168 | tf_op jit(solution)/shard_map/all_gather | solution.py:328
  57.3 0.0 copy-start.1
  57.3 0.0 all-gather.10.cloned.1.call-update
  57.3 0.0 all-gather.6.cloned.1.call-start
  57.4 0.9 dynamic-slice_dynamic-update-slice_fusion.5
  58.3 0.9 dynamic-slice_dynamic-update-slice_fusion.4
  59.3 0.9 dynamic-slice_dynamic-update-slice_fusion.3
  60.2 0.9 dynamic-slice_dynamic-update-slice_fusion.2
  61.2 0.9 dynamic-slice_dynamic-update-slice_fusion.1
  62.1 0.9 dynamic-slice_dynamic-update-slice_fusion
  63.1 0.0 copy-start
  63.1 0.9 copy-done
  64.0 0.0 all-gather.6.cloned.1.call-update
  64.0 0.0 copy-done.2
  64.0 0.6 dynamic_slice.38
  64.6 0.0 copy-done.3
  64.6 0.6 dynamic_slice.36
  65.2 0.8 dynamic-slice_bitcast_fusion
  65.9 5.4 %all-gather.10.cloned.1.call-done = bf16[1,1024,2048]{2,1,0:T(8,128)(2,1)} async-done(((bf16[1,1024,1024]{2,1,0:T(8,128)(2,1)}), bf16[1,1024,2048]{2,1,0:T(8,128)(2,1)}) %all-gather.10.cloned.1.call-update) | async-done | bytes 4194320 | tf_op jit(solution)/shard_map/all_gather | solution.py:329
  71.4 3.1 %fusion = f32[1024]{0:T(1024)S(1)} fusion(bf16[1,1024,2048]{2,1,0:T(8,128)(2,1)} %all-gather.10.cloned.1.call-done), kind=kLoop, calls=%fused_computation.2 | loop fusion | flops 6290432 | bytes 4198400 | tf_op jit(solution)/shard_map/reduce_sum | solution.py:332
  74.4 43.8 %all-gather.6.cloned.1.call-done = bf16[2048,768]{1,0:T(8,128)(2,1)} async-done(((bf16[512,768]{1,0:T(8,128)(2,1)}), bf16[2048,768]{1,0:T(8,128)(2,1)}) %all-gather.6.cloned.1.call-update) | async-done | bytes 3145744 | tf_op jit(solution)/shard_map/all_gather | solution.py:327
  118.3 0.0 copy-done.1
  118.3 6.6 %fusion.9.proj = bf16[1024,768]{1,0:T(8,128)(2,1)S(1)} fusion(bf16[2048,768]{1,0:T(8,128)(2,1)} %all-gather.6.cloned.1.call-done, bf16[1,1024,2048]{2,1,0:T(8,128)(2,1)} %all-gather.10.cloned.1.call-done, f32[2048]{0:T(1024)S(1)} %copy-done.1, f32[1024]{0:T(1024)S(1)} %add_rsqrt_fusion), kind=kOutput, calls=%fused_computation.11 | convolution fusion | flops 3230400512 | bytes 8925184 | tf_op jit(solution)/shard_map/dot_general | solution.py:335
  124.9 5.1 %shard_map.127 = bf16[1024,256]{1,0:T(8,128)(2,1)S(1)} custom-call(bf16[1024,768]{1,0:T(8,128)(2,1)S(1)} %fusion.9.proj, f32[1,1]{1,0:T(1,128)} %bitcast.2.lam_ref, f32[1,128]{1,0:T(1,128)S(1)} %get-tuple-element.6.dgain_ref, f32[1,1]{1,0:T(1,128)} %bitcast.4.rate_ref, f32[1,128]{1,0:T(1,128)S(1)} %get-tuple-element.5.sgain_ref), custom_call_target="tpu_custom_call" | custom-call | tf_op jit(solution)/shard_map/pallas_call | solution.py:299
  130.0 0.3 copy.14
  130.3 19.7 %all_to_all.5 = bf16[8,128,256]{1,2,0:T(8,128)(2,1)S(1)} all-to-all(bf16[8,128,256]{1,2,0:T(8,128)(2,1)S(1)} %copy.14), channel_id=1, replica_groups=mesh['sp'=4,'fs'=4,'tp'=2] {'sp','tp'}, dimensions={0} | all-to-all | bytes 1048576 | tf_op jit(solution)/shard_map/all_to_all | solution.py:338
  150.0 5.5 %fusion.8 = bf16[1,128,2048]{2,1,0:T(8,128)(2,1)} fusion(bf16[128,2048]{0,1:T(8,128)(2,1)S(1)} %bitcast.26, bf16[2048,2048]{1,0:T(8,128)(2,1)} %param.25), kind=kOutput, calls=%fused_computation.10 | convolution fusion | flops 1074003968 | bytes 9437184 | tf_op jit(solution)/shard_map/dot_general | solution.py:344
  (2 shorter events, 0.0 us)
Async XLA Ops:
  6.5 57.4 %copy-start.2 = (f32[4]{0:T(128)S(1)}, f32[4]{0:T(128)}, u32[]{:S(2)}) copy-start(f32[4]{0:T(128)} %param.23) | copy-start | bytes 52
  6.5 58.0 %copy-start.3 = (f32[4]{0:T(128)S(1)}, f32[4]{0:T(128)}, u32[]{:S(2)}) copy-start(f32[4]{0:T(128)} %param.21) | copy-start | bytes 52
  6.5 50.8 %all-gather.8.cloned.1.call-start = ((), (), s32[]{:S(2)}) async-start(), calls=%async_computation.2 | async-start | bytes 2621440 | tf_op jit(solution)/shard_map/all_gather | solution.py:328
  7.3 64.1 %all-gather.10.cloned.1.call-start = ((), (), s32[]{:S(2)}) async-start(), calls=%async_computation.3 | async-start | bytes 6291456 | tf_op jit(solution)/shard_map/all_gather | solution.py:329
  57.3 60.9 %copy-start.1 = (f32[2048]{0:T(1024)S(1)}, f32[2048]{0:T(1024)}, u32[]{:S(2)}) copy-start(f32[2048]{0:T(1024)} %param.14) | copy-start | bytes 24580
  57.3 60.9 %all-gather.6.cloned.1.call-start = ((), (), s32[]{:S(2)}) async-start(), calls=%async_computation.1 | async-start | bytes 3932160 | tf_op jit(solution)/shard_map/all_gather | solution.py:327
  63.1 0.9 copy-start
Sparse Core Ops, SparseCore 0:
  8.9 48.3 all-gather.7
  58.9 12.4 all-gather.9
  73.2 45.0 all-gather.5

commit v2 on v1

--- a/solution.py
+++ b/solution.py
@@ -311,37 +311,360 @@
     )
 
 
+MESH = pl.DeviceIdType.MESH
+
+
+def greet(peers):
+    barrier = pltpu.get_barrier_semaphore()
+    count = 0
+    for peer, present in peers:
+        if present is None:
+            pl.semaphore_signal(barrier, inc=1, device_id=peer, device_id_type=MESH)
+            count = count + 1
+        else:
+
+            @pl.when(present)
+            def _():
+                pl.semaphore_signal(barrier, inc=1, device_id=peer, device_id_type=MESH)
+
+            count = count + jnp.where(present, 1, 0)
+    pl.semaphore_wait(barrier, count)
+
+
+def project_kernel(
+    line,
+    tokens,
+    gain,
+    w0,
+    w1,
+    w2,
+    w3,
+    w4,
+    w5,
+    proj,
+    seq,
+    weight,
+    local_sem,
+    wsend,
+    wrecv,
+    lsend,
+    lrecv,
+    psend,
+    precv,
+):
+    weights = (w0, w1, w2, w3, w4, w5)
+    kinds = len(weights)
+    half_kinds = kinds // 2
+    z, f, c = lax.axis_index("sp"), lax.axis_index("fs"), lax.axis_index("tp")
+    block, half = tokens.shape
+    depth = w0.shape[0]
+    width = weight.shape[1] // kinds
+    near = ({"fs": f ^ 1}, {"fs": f ^ 2})
+    whose = (f ^ 1, f ^ 2, f ^ 3)
+    greet(
+        [
+            (near[0], None),
+            (near[1], None),
+            ({"tp": 1 - c}, None),
+            ({"sp": jnp.minimum(z + 1, line - 1)}, z + 1 < line),
+            ({"sp": jnp.maximum(z - 1, 0)}, z > 0),
+        ]
+    )
+
+    def held(b, side):
+        return seq.at[
+            pl.ds(pl.multiple_of(b * block, block), block),
+            pl.ds(pl.multiple_of(side * half, half), half),
+        ]
+
+    def stored(owner, kind):
+        return weight.at[
+            pl.ds(pl.multiple_of(owner * depth, depth), depth), kind * width : (kind + 1) * width
+        ]
+
+    def slot(e):
+        if isinstance(e, int) and e == 0:
+            return z
+        up = (e - 1) % 2 == 0
+        s = (e - 1) // 2
+        return jnp.where(up, z - 1 - s, z + 1 + s)
+
+    def along(e, b, source=None):
+        up = (e - 1) % 2 == 0
+        target = jnp.where(up, z + 1, z - 1)
+        return pltpu.make_async_remote_copy(
+            src_ref=held(b, c) if source is None else source,
+            dst_ref=held(b, c),
+            send_sem=lsend.at[e],
+            recv_sem=lrecv.at[e],
+            device_id={"sp": jnp.clip(target, 0, line - 1)},
+            device_id_type=MESH,
+        ), (target >= 0) & (target < line)
+
+    def across(e, b, side, source=None):
+        return pltpu.make_async_remote_copy(
+            src_ref=held(b, side) if source is None else source,
+            dst_ref=held(b, side),
+            send_sem=psend.at[e],
+            recv_sem=precv.at[e],
+            device_id={"tp": 1 - c},
+            device_id_type=MESH,
+        )
+
+    for e in (1, 2):
+        copy, present = along(e, z, tokens)
+
+        @pl.when(present)
+        def _():
+            copy.start()
+
+    def own_columns(kind):
+        return weights[kind].at[:, pl.ds(pl.multiple_of(z * width, width), width)]
+
+    def spread(way, kind, source, owner, index):
+        return pltpu.make_async_remote_copy(
+            src_ref=source,
+            dst_ref=stored(owner, kind),
+            send_sem=wsend.at[way, index],
+            recv_sem=wrecv.at[2 if index >= kinds else way, kind],
+            device_id=near[way],
+            device_id_type=MESH,
+        )
+
+    sends = []
+    for turn in range(kinds):
+        for way in range(2):
+            kind = (turn + way * half_kinds) % kinds
+            copy = spread(way, kind, own_columns(kind), f, kind)
+            copy.start()
+            sends.append(copy)
+    across(0, z, c, tokens).start()
+    locals_ = [pltpu.make_async_copy(tokens, held(z, c), local_sem.at[kinds])]
+    for kind in range(kinds):
+        locals_.append(pltpu.make_async_copy(own_columns(kind), stored(f, kind), local_sem.at[kind]))
+    for copy in locals_:
+        copy.start()
+
+    def arrived(relation, kind):
+        pltpu.make_async_remote_copy(
+            src_ref=stored(whose[relation], kind),
+            dst_ref=stored(whose[relation], kind),
+            send_sem=wsend.at[0, kind],
+            recv_sem=wrecv.at[relation, kind],
+            device_id=near[0],
+            device_id_type=MESH,
+        ).wait_recv()
+
+    for turn in range(half_kinds):
+        for way in range(2):
+            kind = turn + way * half_kinds
+            arrived(way, kind)
+            copy = spread(1 - way, kind, stored(whose[way], kind), whose[way], kinds + turn)
+            copy.start()
+            sends.append(copy)
+
+    def take(s):
+        for e in (1 + 2 * s, 2 + 2 * s):
+            b = slot(e)
+
+            @pl.when((b >= 0) & (b < line))
+            def _():
+                copy, _ = along(e, b)
+                copy.wait_recv()
+                if s + 1 < line - 1:
+                    onward, present = along(e + 2, b)
+
+                    @pl.when(present)
+                    def _():
+                        onward.start()
+
+                across(e, b, c).start()
+
+    def process(b):
+        rows = pl.ds(pl.multiple_of(b * block, block), block)
+        x = seq[rows, :].astype(jnp.float32)
+        scaled = x * lax.rsqrt(jnp.mean(x * x, axis=1, keepdims=True) + epsilon)
+        normed = (scaled * gain[...]).astype(jnp.bfloat16)
+        proj[rows, :] = jnp.dot(normed, weight[...], preferred_element_type=jnp.float32).astype(
+            jnp.bfloat16
+        )
+
+    def handle(e, carry):
+        up = (e - 1) % 2 == 0
+        s = (e - 1) // 2
+        b = jnp.where(e == 0, z, jnp.where(up, z - 1 - s, z + 1 + s))
+
+        @pl.when((b >= 0) & (b < line))
+        def _():
+            across(e, b, 1 - c).wait_recv()
+            process(b)
+
+        return carry
+
+    for s in range(line - 2):
+        take(s)
+    for copy in locals_:
+        copy.wait()
+    for kind in range(kinds):
+        for relation in range(3):
+            if relation == 2 or not (relation * half_kinds <= kind < (relation + 1) * half_kinds):
+                arrived(relation, kind)
+    events = 2 * line - 1
+    lax.fori_loop(0, events - 2, handle, 0)
+    take(line - 2)
+    lax.fori_loop(events - 2, events, handle, 0)
+
+    for copy in sends:
+        copy.wait_send()
+    across(0, z, c, tokens).wait_send()
+    for e in (1, 2):
+        copy, present = along(e, z, tokens)
+
+        @pl.when(present)
+        def _():
+            copy.wait_send()
+
+    for s in range(line - 1):
+        for e in (1 + 2 * s, 2 + 2 * s):
+            b = slot(e)
+
+            @pl.when((b >= 0) & (b < line))
+            def _():
+                across(e, b, c).wait_send()
+                if s + 1 < line - 1:
+                    onward, present = along(e + 2, b)
+
+                    @pl.when(present)
+                    def _():
+                        onward.wait_send()
+
+
+def gather_and_project(tokens, norm_gain, weights, line, width):
+    block, half = tokens.shape
+    kinds = len(weights)
+    model = norm_gain.shape[0]
+    anywhere = pl.BlockSpec(memory_space=pl.ANY)
+    vmem = pl.BlockSpec(memory_space=pltpu.VMEM)
+    events = 2 * line - 1
+    dma = pltpu.SemaphoreType.DMA
+    return pl.pallas_call(
+        functools.partial(project_kernel, line),
+        out_shape=jax.ShapeDtypeStruct((line * block, kinds * width), jnp.bfloat16),
+        in_specs=[anywhere, vmem] + [anywhere] * kinds,
+        out_specs=vmem,
+        scratch_shapes=[
+            pltpu.VMEM((line * block, model), jnp.bfloat16),
+            pltpu.VMEM((model, kinds * width), jnp.bfloat16),
+            dma((kinds + 1,)),
+            dma((2, kinds + kinds // 2)),
+            dma((3, kinds)),
+            dma((events,)),
+            dma((events,)),
+            dma((events,)),
+            dma((events,)),
+        ],
+        compiler_params=pltpu.CompilerParams(
+            collective_id=0, has_side_effects=True, vmem_limit_bytes=40 * 1024 * 1024
+        ),
+    )(tokens, norm_gain[None], *weights)
+
+
+def output_kernel(line, pair, mine, out_weight, result, joined, held, wsem, osem, send, recv):
+    z, c = lax.axis_index("sp"), lax.axis_index("tp")
+    count = line * pair
+    me = z * pair + c
+    rows = result.shape[0]
+    width = mine.shape[1] // 2
+    fetch = pltpu.make_async_copy(out_weight, held, wsem)
+    fetch.start()
+    peers = []
+    for turn in range(1, count):
+        other = (me + turn) % count
+        peers.append((other, {"sp": other // pair, "tp": other % pair}))
+    greet([(where, None) for _, where in peers])
+
+    def place(source, which):
+        first = which * (held.shape[0] // 2) + ((source % pair) * line + source // pair) * width
+        return joined.at[:, pl.ds(pl.multiple_of(first, width), width)]
+
+    def piece(target, which):
+        return mine.at[
+            pl.ds(pl.multiple_of(target * rows, rows), rows), which * width : (which + 1) * width
+        ]
+
+    def moved(turn, other, where, which, source):
+        return pltpu.make_async_remote_copy(
+            src_ref=piece(other, which),
+            dst_ref=place(source, which),
+            send_sem=send.at[turn, which],
+            recv_sem=recv.at[turn, which],
+            device_id=where,
+            device_id_type=MESH,
+        )
+
+    for turn, (other, where) in enumerate(peers):
+        for which in range(2):
+            moved(turn, other, where, which, me).start()
+    own = [pltpu.make_async_copy(piece(me, w), place(me, w), osem.at[w]) for w in range(2)]
+    for copy in own:
+        copy.start()
+    for copy in own:
+        copy.wait()
+    fetch.wait()
+    for turn, (other, where) in enumerate(peers):
+        source = (me + count - turn - 1) % count
+        for which in range(2):
+            moved(turn, other, where, which, source).wait_recv()
+    tile = 512
+
+    def one(turn, carry):
+        columns = pl.ds(pl.multiple_of(turn * tile, tile), tile)
+        result[:, columns] = jnp.dot(
+            joined[...], held[:, columns], preferred_element_type=jnp.float32
+        ).astype(jnp.bfloat16)
+        return carry
+
+    lax.fori_loop(0, result.shape[1] // tile, one, 0)
+    for turn, (other, where) in enumerate(peers):
+        for which in range(2):
+            moved(turn, other, where, which, me).wait_send()
+
+
+def exchange_and_output(mine, out_weight, line, pair):
+    count = line * pair
+    rows = mine.shape[0] // count
+    vmem = pl.BlockSpec(memory_space=pltpu.VMEM)
+    dma = pltpu.SemaphoreType.DMA
+    return pl.pallas_call(
+        functools.partial(output_kernel, line, pair),
+        out_shape=jax.ShapeDtypeStruct((rows, out_weight.shape[1]), jnp.bfloat16),
+        in_specs=[vmem, pl.BlockSpec(memory_space=pl.ANY)],
+        out_specs=vmem,
+        scratch_shapes=[
+            pltpu.VMEM((rows, out_weight.shape[0]), jnp.bfloat16),
+            pltpu.VMEM(out_weight.shape, jnp.bfloat16),
+            dma,
+            dma((2,)),
+            dma((count - 1, 2)),
+            dma((count - 1, 2)),
+        ],
+        compiler_params=pltpu.CompilerParams(
+            collective_id=1, has_side_effects=True, vmem_limit_bytes=40 * 1024 * 1024
+        ),
+    )(mine, out_weight)
+
+
 def body(tokens, norm_gain, *rest):
     weights, (map_lambda, diff_gain, decay_rate, state_gain, out_weight) = rest[:6], rest[6:]
-    sp_count = lax.axis_size("sp")
-    tp_count = lax.axis_size("tp")
-    if map_lambda.shape[0] % sp_count or decay_rate.shape[0] != map_lambda.shape[0]:
+    line = lax.axis_size("sp")
+    pair = lax.axis_size("tp")
+    local = map_lambda.shape[0]
+    if local % line or decay_rate.shape[0] != local or lax.axis_size("fs") != 4 or pair != 2:
         return spread_body(tokens, norm_gain, *rest)
-    heads = map_lambda.shape[0] // sp_count
-    block = tokens.shape[1]
-    width = heads * DV
-    place = lax.axis_index("sp")
-    own = jnp.concatenate(
-        [lax.dynamic_slice_in_dim(w, place * width, width, 1) for w in weights], axis=1
-    )
-    weight = lax.all_gather(own, "fs", axis=0, tiled=True)
-    sequence = lax.all_gather(tokens[0], "sp", axis=0, tiled=True)
-    sequence = lax.all_gather(sequence, "tp", axis=1, tiled=True)
-    tok_float = sequence.astype(jnp.float32)
-    normed = tok_float * lax.rsqrt(
-        jnp.mean(tok_float * tok_float, axis=-1, keepdims=True) + epsilon
-    )
-    normed = (normed * norm_gain).astype(jnp.bfloat16)
-    proj = jnp.dot(normed, weight, preferred_element_type=jnp.float32).astype(jnp.bfloat16)
-    mine = mix(proj, block, heads, map_lambda, diff_gain, decay_rate, state_gain)
-    count = sp_count * tp_count
-    moved = lax.all_to_all(
-        mine.reshape(count, mine.shape[0] // count, mine.shape[1]), ("sp", "tp"), 0, 0, tiled=True
-    )
-    rows = moved.shape[1]
-    joined = moved.reshape(sp_count, tp_count, rows, 2, width).transpose(2, 3, 1, 0, 4)
-    joined = joined.reshape(rows, out_weight.shape[0])
-    return jnp.dot(joined, out_weight, preferred_element_type=jnp.float32).astype(jnp.bfloat16)[None]
+    heads = local // line
+    proj = gather_and_project(tokens[0], norm_gain, weights, line, heads * DV)
+    mine = mix(proj, tokens.shape[1], heads, map_lambda, diff_gain, decay_rate, state_gain)
+    return exchange_and_output(mine, out_weight, line, pair)[None]
 
 
 def solution(mesh):

time: 162 us -> 81.2 us (0.50)
  the two profiles are of different devices: /device:TPU:0 before, /device:TPU:15 now
where the time goes in v2:
time: 81.2 us; the launch traced here: 80.7 us
  Pallas kernels  65.2 us (80%)
  local copies, waits for them, and re-layouts  15.5 us (19%)
    pallas_call x1, Pallas kernels, gather_and_project(): pl.pallas_call(functools.partial(project_kernel, line), out_shape=jax.Sha...  36.7 us
    pallas_call x1, Pallas kernels, exchange_and_output(): pl.pallas_call(functools.partial(output_kernel, line, pair), out_shape=ja...  23.3 us
    unnamed x19, local copies, waits for them, and re-layouts  12.2 us
    pallas_call x1, Pallas kernels, mix(): pl.pallas_call(functools.partial(mixers_kernel, block, heads), out_shape=...  5.13 us
    dynamic_slice x2, local copies, waits for them, and re-layouts, own_heads(): return lax.dynamic_slice_in_dim(x, first, heads, 0)[None]  2.52 us

profile of v2, /device:TPU:15, one launch (start us, length us, event | category | flops | bytes accessed | tf_op | source)
XLA Modules:
  0.0 80.7 jit_solution(6918440257274911934)
XLA Ops:
  0.0 1.3 %dynamic_slice.14 = f32[1]{0:T(128)} dynamic-slice(f32[4]{0:T(128)} %param.23, s32[]{:T(128)S(6)} %select_n.8), dynamic_slice_sizes={1} | dynamic-slice | bytes 12 | tf_op jit(solution)/shard_map/dynamic_slice | solution.py:293
  1.3 1.2 %dynamic_slice.12 = f32[1]{0:T(128)} dynamic-slice(f32[4]{0:T(128)} %param.21, s32[]{:T(128)S(6)} %select_n.8), dynamic_slice_sizes={1} | dynamic-slice | bytes 12 | tf_op jit(solution)/shard_map/dynamic_slice | solution.py:293
  2.5 0.8 dynamic-slice_bitcast_fusion
  3.3 0.0 copy-start.1
  3.3 1.0 %copy-done.1 = bf16[1,256,1024]{2,1,0:T(8,128)(2,1)S(1)} copy-done((bf16[1,256,1024]{2,1,0:T(8,128)(2,1)S(1)}, bf16[1,256,1024]{2,1,0:T(8,128)(2,1)}, u32[]{:S(2)}) %copy-start.1) | copy-done | bytes 524312
  4.3 0.0 copy-start.2
  4.3 1.0 %copy-done.2 = bf16[512,512]{1,0:T(8,128)(2,1)S(1)} copy-done((bf16[512,512]{1,0:T(8,128)(2,1)S(1)}, bf16[512,512]{1,0:T(8,128)(2,1)}, u32[]{:S(2)}) %copy-start.2) | copy-done | bytes 524312
  5.4 0.0 copy-start.3
  5.4 1.0 %copy-done.3 = bf16[512,512]{1,0:T(8,128)(2,1)S(1)} copy-done((bf16[512,512]{1,0:T(8,128)(2,1)S(1)}, bf16[512,512]{1,0:T(8,128)(2,1)}, u32[]{:S(2)}) %copy-start.3) | copy-done | bytes 524312
  6.4 0.0 copy-start.4
  6.4 1.0 %copy-done.4 = bf16[512,512]{1,0:T(8,128)(2,1)S(1)} copy-done((bf16[512,512]{1,0:T(8,128)(2,1)S(1)}, bf16[512,512]{1,0:T(8,128)(2,1)}, u32[]{:S(2)}) %copy-start.4) | copy-done | bytes 524312
  7.5 0.0 copy-start.5
  7.5 1.0 %copy-done.5 = bf16[512,512]{1,0:T(8,128)(2,1)S(1)} copy-done((bf16[512,512]{1,0:T(8,128)(2,1)S(1)}, bf16[512,512]{1,0:T(8,128)(2,1)}, u32[]{:S(2)}) %copy-start.5) | copy-done | bytes 524312
  8.5 0.0 copy-start.6
  8.5 1.0 %copy-done.6 = bf16[512,512]{1,0:T(8,128)(2,1)S(1)} copy-done((bf16[512,512]{1,0:T(8,128)(2,1)S(1)}, bf16[512,512]{1,0:T(8,128)(2,1)}, u32[]{:S(2)}) %copy-start.6) | copy-done | bytes 524312
  9.6 0.0 copy-start.7
  9.6 1.0 %copy-done.7 = bf16[512,512]{1,0:T(8,128)(2,1)S(1)} copy-done((bf16[512,512]{1,0:T(8,128)(2,1)S(1)}, bf16[512,512]{1,0:T(8,128)(2,1)}, u32[]{:S(2)}) %copy-start.7) | copy-done | bytes 524312
  10.6 0.0 copy-start.8
  10.6 0.7 copy-done.8
  11.3 36.7 %shard_map.127.proj = bf16[1024,768]{1,0:T(8,128)(2,1)S(1)} custom-call(bf16[256,1024]{1,0:T(8,128)(2,1)S(1)} %bitcast.10, f32[1,2048]{1,0:T(1,128)S(1)} %bitcast.11, bf16[512,512]{1,0:T(8,128)(2,1)S(1)} %copy-done.2, bf16[512,512]{1,0:T(8,128)(2,1)S(1)} %copy-done.3, bf16[512,512]{1,0:T(8,128)(2,1)S(1)} %copy-done.4, bf16[512,512]{1,0:T(8,128)(2,1)S(1)} %copy-done.5, ...), custom_call_target="tpu_custom_call" | custom-call | tf_op jit(solution)/shard_map/pallas_call | solution.py:550
  48.0 5.1 %shard_map.128.mine = bf16[1024,256]{1,0:T(8,128)(2,1)S(1)} custom-call(bf16[1024,768]{1,0:T(8,128)(2,1)S(1)} %shard_map.127.proj, f32[1,1]{1,0:T(1,128)} %bitcast.2.lam_ref, f32[1,128]{1,0:T(1,128)S(1)} %get-tuple-element.6.dgain_ref, f32[1,1]{1,0:T(1,128)} %bitcast.4.rate_ref, f32[1,128]{1,0:T(1,128)S(1)} %get-tuple-element.5.sgain_ref), custom_call_target="tpu_custom_call" | custom-call | tf_op jit(solution)/shard_map/pallas_call | solution.py:299
  53.2 0.0 copy-start
  53.2 3.4 %copy-done = bf16[2048,2048]{1,0:T(8,128)(2,1)S(1)} copy-done((bf16[2048,2048]{1,0:T(8,128)(2,1)S(1)}, bf16[2048,2048]{1,0:T(8,128)(2,1)}, u32[]{:S(2)}) %copy-start) | copy-done | bytes 8388632
  56.5 23.3 %shard_map.129 = bf16[128,2048]{1,0:T(8,128)(2,1)S(1)} custom-call(bf16[1024,256]{1,0:T(8,128)(2,1)S(1)} %shard_map.128.mine, bf16[2048,2048]{1,0:T(8,128)(2,1)S(1)} %copy-done), custom_call_target="tpu_custom_call" | custom-call | tf_op jit(solution)/shard_map/pallas_call | solution.py:638
  79.9 0.8 copy.15
Async XLA Ops:
  3.3 1.0 %copy-start.1 = (bf16[1,256,1024]{2,1,0:T(8,128)(2,1)S(1)}, bf16[1,256,1024]{2,1,0:T(8,128)(2,1)}, u32[]{:S(2)}) copy-start(bf16[1,256,1024]{2,1,0:T(8,128)(2,1)} %param.13) | copy-start | bytes 1572868
  4.3 1.0 %copy-start.2 = (bf16[512,512]{1,0:T(8,128)(2,1)S(1)}, bf16[512,512]{1,0:T(8,128)(2,1)}, u32[]{:S(2)}) copy-start(bf16[512,512]{1,0:T(8,128)(2,1)} %w0.1) | copy-start | bytes 1572868
  5.4 1.0 %copy-start.3 = (bf16[512,512]{1,0:T(8,128)(2,1)S(1)}, bf16[512,512]{1,0:T(8,128)(2,1)}, u32[]{:S(2)}) copy-start(bf16[512,512]{1,0:T(8,128)(2,1)} %w1.1) | copy-start | bytes 1572868
  6.4 1.0 %copy-start.4 = (bf16[512,512]{1,0:T(8,128)(2,1)S(1)}, bf16[512,512]{1,0:T(8,128)(2,1)}, u32[]{:S(2)}) copy-start(bf16[512,512]{1,0:T(8,128)(2,1)} %w2.1) | copy-start | bytes 1572868
  7.5 1.0 %copy-start.5 = (bf16[512,512]{1,0:T(8,128)(2,1)S(1)}, bf16[512,512]{1,0:T(8,128)(2,1)}, u32[]{:S(2)}) copy-start(bf16[512,512]{1,0:T(8,128)(2,1)} %w3.1) | copy-start | bytes 1572868
  8.5 1.0 %copy-start.6 = (bf16[512,512]{1,0:T(8,128)(2,1)S(1)}, bf16[512,512]{1,0:T(8,128)(2,1)}, u32[]{:S(2)}) copy-start(bf16[512,512]{1,0:T(8,128)(2,1)} %w4.1) | copy-start | bytes 1572868
  9.6 1.0 %copy-start.7 = (bf16[512,512]{1,0:T(8,128)(2,1)S(1)}, bf16[512,512]{1,0:T(8,128)(2,1)}, u32[]{:S(2)}) copy-start(bf16[512,512]{1,0:T(8,128)(2,1)} %w5.1) | copy-start | bytes 1572868
  10.6 0.7 copy-start.8
  53.2 3.4 %copy-start = (bf16[2048,2048]{1,0:T(8,128)(2,1)S(1)}, bf16[2048,2048]{1,0:T(8,128)(2,1)}, u32[]{:S(2)}) copy-start(bf16[2048,2048]{1,0:T(8,128)(2,1)} %out_weight.1) | copy-start | bytes 25165828

commit v3 on v2

--- a/solution.py
+++ b/solution.py
@@ -224,6 +224,7 @@
 def mixers_kernel(block, heads, proj, lam_ref, dgain_ref, rate_ref, sgain_ref, out):
     length = proj.shape[0]
     group = heads * DV
+    place = lax.axis_index("sp")
     f32, bf16 = jnp.float32, jnp.bfloat16
     row = lax.broadcasted_iota(jnp.int32, (block, block), 0)
     col = lax.broadcasted_iota(jnp.int32, (block, block), 1)
@@ -236,13 +237,14 @@
 
     for head in range(heads):
         spot = slice(head * DV, head * DV + DV)
-        lam = lam_ref[:, head : head + 1]
-        rate = rate_ref[:, head : head + 1]
-        gain = dgain_ref[:, spot] * branch_scale
+        lam = lam_ref[place * heads + head]
+        rate = rate_ref[place * heads + head]
+        mine = pl.ds(pl.multiple_of((place * heads + head) * DV, DV), DV)
+        gain = dgain_ref[:, mine] * branch_scale
         within = jnp.where(causal, jnp.exp(-rate * jnp.maximum(row - col, 0).astype(f32)), 0.0)
         query_decay = jnp.exp(-rate * (position + 1.0))
         key_decay = jnp.exp(-rate * (block - 1.0 - position))
-        block_decay = jnp.exp(-rate * block)
+        block_decay = jnp.exp(jnp.full((1, DR), -block, f32) * rate)
         state = jnp.zeros((DR, DR), f32)
         for turn in range(length // block):
             first = turn * block
@@ -284,30 +286,26 @@
                 )
             scaled = mixed * lax.rsqrt(jnp.mean(mixed * mixed, axis=1, keepdims=True) + epsilon)
             out[first : first + block, group + head * DV : group + head * DV + DV] = (
-                scaled * sgain_ref[:, spot]
+                scaled * sgain_ref[:, mine]
             ).astype(bf16)
-
-
-def own_heads(x, heads):
-    first = lax.axis_index("sp") * heads
-    return lax.dynamic_slice_in_dim(x, first, heads, 0)[None]
 
 
 def mix(proj, block, heads, map_lambda, diff_gain, decay_rate, state_gain):
     length = proj.shape[0]
     vmem = pl.BlockSpec(memory_space=pltpu.VMEM)
+    smem = pl.BlockSpec(memory_space=pltpu.SMEM)
     return pl.pallas_call(
         functools.partial(mixers_kernel, block, heads),
         out_shape=jax.ShapeDtypeStruct((length, 2 * heads * DV), jnp.bfloat16),
-        in_specs=[vmem] * 5,
+        in_specs=[vmem, smem, vmem, smem, vmem],
         out_specs=vmem,
-        compiler_params=pltpu.CompilerParams(vmem_limit_bytes=48 * 1024 * 1024),
+        compiler_params=pltpu.CompilerParams(vmem_limit_bytes=65000 * 1024),
     )(
         proj,
-        own_heads(map_lambda, heads),
-        own_heads(diff_gain, heads * DV),
-        own_heads(decay_rate, heads),
-        own_heads(state_gain, heads * DR),
+        map_lambda,
+        diff_gain[None],
+        decay_rate,
+        state_gain[None],
     )
 
 
@@ -564,7 +562,7 @@
             dma((events,)),
         ],
         compiler_params=pltpu.CompilerParams(
-            collective_id=0, has_side_effects=True, vmem_limit_bytes=40 * 1024 * 1024
+            collective_id=0, has_side_effects=True, vmem_limit_bytes=65000 * 1024
         ),
     )(tokens, norm_gain[None], *weights)
 
@@ -649,7 +647,7 @@
             dma((count - 1, 2)),
         ],
         compiler_params=pltpu.CompilerParams(
-            collective_id=1, has_side_effects=True, vmem_limit_bytes=40 * 1024 * 1024
+            collective_id=1, has_side_effects=True, vmem_limit_bytes=65000 * 1024
         ),
     )(mine, out_weight)
 

time: 81.2 us -> 71.6 us (0.88)
  local copies, waits for them, and re-layouts: 15.5 us -> 1.88 us
  Pallas kernels: 65.2 us -> 69.4 us
    unnamed x19 -> x1, local copies, waits for them, and re-layouts: 12.2 us -> 1.88 us
    dynamic_slice x2 -> x0, local copies, waits for them, and re-layouts: 2.52 us -> none  [own_heads(): return lax.dynamic_slice_in_dim(x, first, heads, 0)[None]]
    pallas_call x1, Pallas kernels: 36.7 us -> 38.8 us  [gather_and_project(): pl.pallas_call(functools.partial(project_kernel, line), out_shape=jax.Sha...]
    pallas_call x1, Pallas kernels: 23.3 us -> 24.5 us  [exchange_and_output(): pl.pallas_call(functools.partial(output_kernel, line, pair), out_shape=ja...]
    pallas_call x1, Pallas kernels: 5.13 us -> 6.1 us  [mix(): pl.pallas_call(functools.partial(mixers_kernel, block, heads), out_shape=...]
where the time goes in v3:
time: 71.6 us; the launch traced here: 71.3 us
  Pallas kernels  69.4 us (97%)
  local copies, waits for them, and re-layouts  1.88 us (3%)
    pallas_call x1, Pallas kernels, gather_and_project(): pl.pallas_call(functools.partial(project_kernel, line), out_shape=jax.Sha...  38.8 us
    pallas_call x1, Pallas kernels, exchange_and_output(): pl.pallas_call(functools.partial(output_kernel, line, pair), out_shape=ja...  24.5 us
    pallas_call x1, Pallas kernels, mix(): pl.pallas_call(functools.partial(mixers_kernel, block, heads), out_shape=...  6.1 us
    unnamed x1, local copies, waits for them, and re-layouts  1.88 us

profile of v3, /device:TPU:15, one launch (start us, length us, event | category | flops | bytes accessed | tf_op | source)
XLA Modules:
  0.0 71.3 jit_solution(2601591444420197141)
XLA Ops:
  0.0 38.8 %shard_map.127.proj = bf16[1024,768]{1,0:T(8,128)(2,1)} custom-call(bf16[256,1024]{1,0:T(8,128)(2,1)} %bitcast.6, f32[1,2048]{1,0:T(1,128)} %bitcast.7, bf16[512,512]{1,0:T(8,128)(2,1)} %w0.1, bf16[512,512]{1,0:T(8,128)(2,1)} %w1.1, bf16[512,512]{1,0:T(8,128)(2,1)} %w2.1, bf16[512,512]{1,0:T(8,128)(2,1)} %w3.1, bf16[512,512]{1,0:T(8,128)(2,1)} %w4.1, ...), custom_call_target="tpu_custom_call" | custom-call | tf_op jit(solution)/shard_map/pallas_call | solution.py:548
  38.8 6.1 %shard_map.128.mine = bf16[1024,256]{1,0:T(8,128)(2,1)} custom-call(bf16[1024,768]{1,0:T(8,128)(2,1)} %shard_map.127.proj, f32[4]{0:T(128)} %lam_ref.1, f32[1,512]{1,0:T(1,128)} %bitcast.8, f32[4]{0:T(128)} %rate_ref.1, f32[1,512]{1,0:T(1,128)} %bitcast.9), custom_call_target="tpu_custom_call" | custom-call | tf_op jit(solution)/shard_map/pallas_call | solution.py:297
  44.9 24.5 %shard_map.129 = bf16[128,2048]{1,0:T(8,128)(2,1)} custom-call(bf16[1024,256]{1,0:T(8,128)(2,1)} %shard_map.128.mine, bf16[2048,2048]{1,0:T(8,128)(2,1)} %out_weight.1), custom_call_target="tpu_custom_call" | custom-call | tf_op jit(solution)/shard_map/pallas_call | solution.py:636
  69.4 1.9 %copy.15 = bf16[1,128,2048]{2,1,0:T(8,128)(2,1)} copy(bf16[1,128,2048]{2,1,0:T(8,128)(2,1)} %bitcast.5) | data formatting | bytes 1048576
